TPU v7x, 32 devices: a whole 2x2x4 slice. The times are simulated.
32 devices in a mesh: fs: 8 (over z, x), tp: 4 (over y, core).
Axes of the slice: x: 2, y: 2, z: 4, core: 2. Of those that a mesh axis runs over, the one named last changes fastest.
Arguments:
- later_in: bfloat16 [8192, 2048], P('fs'), may hold values from -3 to 3
- earlier_in: bfloat16 [8192, 2048], P('fs'), may hold values from -3 to 3
- cotangent: bfloat16 [8192, 2048], P('fs'), may hold values from -6 to 6
- gate_weight: bfloat16 [2048, 5632], P('fs', 'tp'), may hold values from -0.125 to 0.125
- up_weight: bfloat16 [2048, 5632], P('fs', 'tp'), may hold values from -0.125 to 0.125
- down_weight: bfloat16 [2048, 5632], P('fs', 'tp'), may hold values from -0.078125 to 0.078125
- norm_gain: bfloat16 [2048], replicated, may hold values from 0.099609375 to 1.8984375
- gate_sum: float32 [2048, 5632], P('fs', 'tp'), may hold values from -96 to 96
- up_sum: float32 [2048, 5632], P('fs', 'tp'), may hold values from -96 to 96
- down_sum: float32 [2048, 5632], P('fs', 'tp'), may hold values from -96 to 96
- gain_sum: float32 [2048], replicated, may hold values from -192 to 192
Outputs:
- later_out: bfloat16 [8192, 2048], P(('fs', 'tp'))
- later_hidden: bfloat16 [8192, 5632], P('fs', 'tp')
- earlier_grad: bfloat16 [8192, 2048], P(('fs', 'tp'))
- gate_sum_new: float32 [2048, 5632], P('fs', 'tp')
- up_sum_new: float32 [2048, 5632], P('fs', 'tp')
- down_sum_new: float32 [2048, 5632], P('fs', 'tp')
- gain_sum_new: float32 [2048], replicated
All inputs are finite; a program needn't handle non-finite values.
Results may differ from a plain program's by a relative error of at most 0.013.
Values may be sent and summed in bfloat16 or wider, within the bound.
No kernel may reach another device: no remote copies, remote signals or barrier semaphores. Data moves between devices by JAX's collectives and lax.ppermute only.
A program may use at most 128 MiB of HBM per device.

v0:
```python
import jax
import jax.numpy as jnp
from jax import lax
from jax.sharding import PartitionSpec as P

norm_floor = 0.05


def normalize(tokens_in, norm_gain):
    values = tokens_in.astype(jnp.float32)
    row_scale = lax.rsqrt(jnp.mean(values * values, axis=1, keepdims=True) + norm_floor)
    unit_rows = values * row_scale
    normed = (unit_rows * norm_gain.astype(jnp.float32)).astype(jnp.bfloat16)
    return (row_scale, unit_rows, normed)


def transposed(matrix_a, matrix_b):
    return lax.dot_general(
        matrix_a, matrix_b, (((1,), (1,)), ((), ())), preferred_element_type=jnp.float32
    )


def outer_sum(matrix_a, matrix_b):
    return lax.dot_general(
        matrix_a, matrix_b, (((0,), (0,)), ((), ())), preferred_element_type=jnp.float32
    )


def own_rows(tokens_in, own_count):
    return lax.dynamic_slice_in_dim(tokens_in, lax.axis_index("tp") * own_count, own_count, 0)


def forward(later_in, norm_gain, weights):
    w_gate, w_up, w_down = weights
    normed = normalize(later_in, norm_gain)[2]
    gate_pre = jnp.dot(normed, w_gate, preferred_element_type=jnp.float32)
    up_pre = jnp.dot(normed, w_up, preferred_element_type=jnp.float32)
    hidden = (jax.nn.silu(gate_pre) * up_pre).astype(jnp.bfloat16)
    own_count = later_in.shape[0] // lax.axis_size("tp")
    summed = lax.psum_scatter(
        transposed(hidden, w_down).astype(jnp.bfloat16), "tp", scatter_dimension=0, tiled=True
    ).astype(jnp.float32)
    later_out = (own_rows(later_in, own_count).astype(jnp.float32) + 0.5 * summed).astype(
        jnp.bfloat16
    )
    return (later_out, hidden)


def backward(earlier_in, cotangent, norm_gain, weights):
    w_gate, w_up, w_down = weights
    row_scale, unit_rows, normed = normalize(earlier_in, norm_gain)
    gate_pre = jnp.dot(normed, w_gate, preferred_element_type=jnp.float32)
    up_pre = jnp.dot(normed, w_up, preferred_element_type=jnp.float32)
    sigmoid_gate = jax.nn.sigmoid(gate_pre)
    activated = gate_pre * sigmoid_gate
    hidden = (activated * up_pre).astype(jnp.bfloat16)
    col_width = hidden.shape[1]
    dhidden = jnp.dot(cotangent, w_down, preferred_element_type=jnp.float32)
    dgate = (
        0.5 * dhidden * up_pre * sigmoid_gate * (1.0 + gate_pre * (1.0 - sigmoid_gate))
    ).astype(jnp.bfloat16)
    dupper = (0.5 * dhidden * activated).astype(jnp.bfloat16)
    gate_and_up = jnp.concatenate([dgate, dupper], axis=1)
    dnormed = transposed(dgate, w_gate) + transposed(dupper, w_up)
    gain_part = jnp.sum(dnormed * unit_rows, axis=0)
    weighted = dnormed * norm_gain.astype(jnp.float32)
    branch = row_scale * (
        weighted - unit_rows * jnp.mean(weighted * unit_rows, axis=1, keepdims=True)
    )
    own_count = earlier_in.shape[0] // lax.axis_size("tp")
    summed = lax.psum_scatter(
        branch.astype(jnp.bfloat16), "tp", scatter_dimension=0, tiled=True
    ).astype(jnp.float32)
    earlier_grad = (own_rows(cotangent, own_count).astype(jnp.float32) + summed).astype(
        jnp.bfloat16
    )
    grads_total = lax.psum_scatter(
        jnp.concatenate(
            [outer_sum(normed, gate_and_up), 0.5 * outer_sum(cotangent, hidden)], axis=1
        ).astype(jnp.bfloat16),
        "fs",
        scatter_dimension=0,
        tiled=True,
    ).astype(jnp.float32)
    grad_gate = grads_total[:, :col_width]
    grad_up = grads_total[:, col_width : 2 * col_width]
    grad_down = grads_total[:, 2 * col_width :]
    gain_total = lax.psum(gain_part, ("fs", "tp"))
    return (earlier_grad, grad_gate, grad_up, grad_down, gain_total)


def local(
    later_in,
    earlier_in,
    cotangent,
    gate_weight,
    up_weight,
    down_weight,
    norm_gain,
    gate_sum,
    up_sum,
    down_sum,
    gain_sum,
):
    pieces = (gate_weight, up_weight, down_weight)
    later_out, later_hidden = forward(
        later_in,
        norm_gain,
        (
            lax.all_gather(pieces[0], "fs", axis=0, tiled=True),
            lax.all_gather(pieces[1], "fs", axis=0, tiled=True),
            lax.all_gather(pieces[2], "fs", axis=0, tiled=True),
        ),
    )
    earlier = backward(
        earlier_in,
        cotangent,
        norm_gain,
        (
            lax.all_gather(pieces[0], "fs", axis=0, tiled=True),
            lax.all_gather(pieces[1], "fs", axis=0, tiled=True),
            lax.all_gather(pieces[2], "fs", axis=0, tiled=True),
        ),
    )
    earlier_grad, grad_gate, grad_up, grad_down, gain_total = earlier
    return (
        later_out,
        later_hidden,
        earlier_grad,
        gate_sum + grad_gate,
        up_sum + grad_up,
        down_sum + grad_down,
        gain_sum + gain_total,
    )


def solution(mesh):
    placed = (
        P("fs", None),
        P("fs", None),
        P("fs", None),
        P("fs", "tp"),
        P("fs", "tp"),
        P("fs", "tp"),
        P(),
        P("fs", "tp"),
        P("fs", "tp"),
        P("fs", "tp"),
        P(),
    )
    return jax.shard_map(
        local,
        mesh=mesh,
        in_specs=placed,
        out_specs=(
            P(("fs", "tp"), None),
            P("fs", "tp"),
            P(("fs", "tp"), None),
            P("fs", "tp"),
            P("fs", "tp"),
            P("fs", "tp"),
            P(),
        ),
        check_vma=False,
    )
```

profile of v0, /device:TPU:0, one launch (start us, length us, event | category | flops | bytes accessed | tf_op | source)
XLA Modules:
  0.0 708.4 jit_solution(3213249192349217438)
XLA Ops:
  7.2 0.7 all-gather.4.cloned.1.call-update
  7.9 0.7 all-gather.6.cloned.1.call-update
  8.7 0.0 all-gather.8.cloned.1.call-start
  8.7 0.7 all-gather.8.cloned.1.call-update
  9.4 0.0 reduce-scatter.4.cloned.1.call-start
  9.4 0.8 convert_element_type.59
  10.3 3.3 fusion.4
  13.6 0.9 fusion.13
  14.5 90.8 %all-gather.4.cloned.1.call-done = bf16[2048,1408]{1,0:T(8,128)(2,1)} async-done(((bf16[256,1408]{1,0:T(8,128)(2,1)}), bf16[2048,1408]{1,0:T(8,128)(2,1)}) %all-gather.4.cloned.1.call-update) | async-done | bytes 5767184 | tf_op jit(solution)/shard_map/all_gather | solution.py:110
  105.2 12.0 %fusion.20 = f32[1024,1408]{1,0:T(8,128)} fusion(bf16[2048,1408]{1,0:T(8,128)(2,1)} %all-gather.4.cloned.1.call-done, bf16[1024,2048]{1,0:T(8,128)(2,1)} %param.11, f32[2048]{0:T(1024)S(1)} %convert_element_type.59, f32[1024]{0:T(1024)S(1)} %add_rsqrt_fusion.1), kind=kOutput, calls=%fused_computation.38 | convolution fusion | flops 5913968640 | bytes 15740928 | tf_op jit(solution)/shard_map/dot_general | solution.py:36
  117.2 80.8 %all-gather.6.cloned.1.call-done = bf16[2048,1408]{1,0:T(8,128)(2,1)} async-done(((bf16[256,1408]{1,0:T(8,128)(2,1)}), bf16[2048,1408]{1,0:T(8,128)(2,1)}) %all-gather.6.cloned.1.call-update) | async-done | bytes 5767184 | tf_op jit(solution)/shard_map/all_gather | solution.py:111
  197.9 11.3 %multiply_convert_fusion.4 = bf16[1024,1408]{1,0:T(8,128)(2,1)S(1)} fusion(f32[1024,1408]{1,0:T(8,128)} %fusion.20, bf16[2048,1408]{1,0:T(8,128)(2,1)} %all-gather.6.cloned.1.call-done, bf16[1024,2048]{1,0:T(8,128)(2,1)} %param.11, f32[2048]{0:T(1024)S(1)} %convert_element_type.59, f32[1024]{0:T(1024)S(1)} %add_rsqrt_fusion.1), kind=kOutput, calls=%fused_computation.30 | convolution fusion | flops 5922619392 | bytes 18624512 | tf_op jit(solution)/shard_map/dot_general | solution.py:37
  209.3 81.4 %all-gather.8.cloned.1.call-done = bf16[2048,1408]{1,0:T(8,128)(2,1)} async-done(((bf16[256,1408]{1,0:T(8,128)(2,1)}), bf16[2048,1408]{1,0:T(8,128)(2,1)}) %all-gather.8.cloned.1.call-update) | async-done | bytes 5767184 | tf_op jit(solution)/shard_map/all_gather | solution.py:112
  290.6 10.9 %convolution_convert_fusion.1 = bf16[1024,2048]{1,0:T(8,128)(2,1)} fusion(bf16[1024,1408]{1,0:T(8,128)(2,1)S(1)} %multiply_convert_fusion.4, bf16[2048,1408]{1,0:T(8,128)(2,1)} %all-gather.8.cloned.1.call-done), kind=kOutput, calls=%fused_computation.32 | convolution fusion | flops 5907677184 | bytes 12845056 | tf_op jit(solution)/shard_map/dot_general | solution.py:18
  301.5 0.2 reduce-scatter.6.cloned.1.call-start
  301.8 12.1 %fusion.26 = f32[1024,1408]{1,0:T(8,128)} fusion(bf16[2048,1408]{1,0:T(8,128)(2,1)} %all-gather.4.cloned.1.call-done, bf16[1024,2048]{1,0:T(8,128)(2,1)} %param.12, f32[1024]{0:T(1024)S(1)} %add_rsqrt_fusion, f32[2048]{0:T(1024)S(1)} %convert_element_type.59), kind=kOutput, calls=%fused_computation.44 | convolution fusion | flops 5913968640 | bytes 15740928 | tf_op jit(solution)/shard_map/dot_general | solution.py:52
  313.9 10.7 %fusion.28 = f32[1024,1408]{1,0:T(8,128)} fusion(bf16[2048,1408]{1,0:T(8,128)(2,1)} %all-gather.6.cloned.1.call-done, bf16[1024,2048]{1,0:T(8,128)(2,1)S(1)} %copy-done.1, f32[1024]{0:T(1024)S(1)} %add_rsqrt_fusion, f32[2048]{0:T(1024)S(1)} %convert_element_type.59), kind=kOutput, calls=%fused_computation.45 | convolution fusion | flops 5913968640 | bytes 15740928 | tf_op jit(solution)/shard_map/dot_general | solution.py:53
  324.7 12.3 %multiply_convert_fusion.2 = (bf16[1024,1408]{1,0:T(8,128)(2,1)S(1)}, bf16[1024,1408]{1,0:T(8,128)(2,1)}) fusion(f32[1024,1408]{1,0:T(8,128)} %fusion.26, f32[1024,1408]{1,0:T(8,128)} %fusion.28, bf16[1024,2048]{1,0:T(8,128)(2,1)S(1)} %copy-done.6, bf16[2048,1408]{1,0:T(8,128)(2,1)S(1)} %bitcast.18), kind=kOutput, calls=%fused_computation.26 | convolution fusion | flops 5925765120 | bytes 27262976 | tf_op jit(solution)/shard_map/dot_general | solution.py:58
  337.0 10.2 %fusion.30 = f32[1024,2048]{1,0:T(8,128)} fusion(bf16[1024,1408]{1,0:T(8,128)(2,1)} %get-tuple-element.10, bf16[2048,1408]{1,0:T(8,128)(2,1)S(1)} %bitcast.16), kind=kOutput, calls=%fused_computation.46 | convolution fusion | flops 5905580032 | bytes 17039360 | tf_op jit(solution)/shard_map/dot_general | solution.py:18
  347.2 11.1 %fusion.12 = (f32[2048]{0:T(1024)S(1)}, f32[1024]{0:T(1024)S(1)}, f32[1024,2048]{1,0:T(8,128)S(1)}) fusion(bf16[1024,2048]{1,0:T(8,128)(2,1)S(1)} %copy-done.1, f32[1024]{0:T(1024)S(1)} %add_rsqrt_fusion, f32[2048]{0:T(1024)S(1)} %convert_element_type.59, f32[1024,2048]{1,0:T(8,128)} %fusion.30, bf16[1024,1408]{1,0:T(8,128)(2,1)S(1)} %get-tuple-element.9, ...), kind=kOutput, calls=%fused_computation.19 | convolution fusion | flops 5922354176 | bytes 29646848 | tf_op jit(solution)/shard_map/dot_general | solution.py:18
  358.3 3.5 fusion.11
  361.9 0.0 reduce-scatter.8.cloned.1.call-start
  361.9 13.0 %fusion.14 = bf16[2048,1408]{1,0:T(8,128)(2,1)S(1)} fusion(bf16[1024,2048]{1,0:T(8,128)(2,1)} %param.13, f32[1024,1408]{1,0:T(8,128)} %fusion.28, f32[1024,1408]{1,0:T(8,128)} %fusion.26), kind=kOutput, calls=%fused_computation.21 | convolution fusion | flops 5919997952 | bytes 21495808 | tf_op jit(solution)/shard_map/dot_general | solution.py:24
  374.9 17.4 %convolution_convert_fusion = bf16[2048,2816]{1,0:T(8,128)(2,1)} fusion(bf16[1024,1408]{1,0:T(8,128)(2,1)S(1)} %get-tuple-element.9, bf16[1024,1408]{1,0:T(8,128)(2,1)} %get-tuple-element.10, bf16[1024,2048]{1,0:T(8,128)(2,1)S(1)} %copy-done.2, f32[1024]{0:T(1024)S(1)} %add_rsqrt_fusion, f32[2048]{0:T(1024)S(1)} %convert_element_type.59), kind=kOutput, calls=%fused_computation.2 | convolution fusion | flops 11836850176 | bytes 21508096 | tf_op jit(solution)/shard_map/dot_general | solution.py:24
  392.3 11.8 %pad_maximum_fusion = bf16[2048,4224]{1,0:T(8,128)(2,1)} fusion(bf16[2048,1408]{1,0:T(8,128)(2,1)S(1)} %fusion.14, bf16[2048,2816]{1,0:T(8,128)(2,1)} %convolution_convert_fusion), kind=kLoop, calls=%fused_computation | loop fusion | flops 34603008 | bytes 34603008 | tf_op jit(solution)/shard_map/concatenate | solution.py:78
  404.1 41.4 %psum.7 = f32[2048]{0:T(1024)S(1)} all-reduce(f32[2048]{0:T(1024)S(1)} %get-tuple-element.7), channel_id=1, replica_groups=mesh['fs'=8,'tp'=4] {'fs','tp'}, use_global_device_ids=true, to_apply=%region_7.8 | all-reduce | flops 2048 | bytes 16384 | tf_op jit(solution)/shard_map/psum | solution.py:88
  445.5 0.6 add.71
  446.1 3.1 add_convert_fusion.1
  449.2 2.9 add_convert_fusion
  452.2 245.1 %reduce-scatter.8.cloned.1.call-done = bf16[256,4224]{1,0:T(8,128)(2,1)} async-done(((bf16[2048,4224]{1,0:T(8,128)(2,1)}), bf16[256,4224]{1,0:T(8,128)(2,1)}) %reduce-scatter.8.cloned.1.call-update) | async-done | bytes 2162704 | tf_op jit(solution)/shard_map/reduce_scatter | solution.py:77
  697.2 2.0 convert_element_type.74
  699.3 2.3 slice_add_fusion
  (38 shorter events, 0.2 us)
Async XLA Ops:
  7.2 98.1 %all-gather.4.cloned.1.call-start = ((), (), s32[]{:S(2)}) async-start(), calls=%async_computation.3 | async-start | bytes 6488064 | tf_op jit(solution)/shard_map/all_gather | solution.py:110
  7.9 190.0 %all-gather.6.cloned.1.call-start = ((), (), s32[]{:S(2)}) async-start(), calls=%async_computation.4 | async-start | bytes 6488064 | tf_op jit(solution)/shard_map/all_gather | solution.py:111
  8.7 282.0 %all-gather.8.cloned.1.call-start = ((), (), s32[]{:S(2)}) async-start(), calls=%async_computation.5 | async-start | bytes 6488064 | tf_op jit(solution)/shard_map/all_gather | solution.py:112
  9.4 436.8 %reduce-scatter.4.cloned.1.call-start = ((), (), s32[]{:S(2)}) async-start(), calls=%async_computation.6 | async-start | bytes 5242880 | tf_op jit(solution)/shard_map/reduce_scatter | solution.py:40
  9.4 4.1 copy-start
  209.2 92.3 %copy-start.8 = (bf16[1024,1408]{1,0:T(8,128)(2,1)}, bf16[1024,1408]{1,0:T(8,128)(2,1)S(1)}, u32[]{:S(2)}) copy-start(bf16[1024,1408]{1,0:T(8,128)(2,1)S(1)} %multiply_convert_fusion.4) | copy-start | bytes 8650756
  301.5 147.7 %reduce-scatter.6.cloned.1.call-start = ((), (), s32[]{:S(2)}) async-start(), calls=%async_computation.7 | async-start | bytes 5242880 | tf_op jit(solution)/shard_map/reduce_scatter | solution.py:71
  301.8 12.2 %copy-start.1 = (bf16[1024,2048]{1,0:T(8,128)(2,1)S(1)}, bf16[1024,2048]{1,0:T(8,128)(2,1)}, u32[]{:S(2)}) copy-start(bf16[1024,2048]{1,0:T(8,128)(2,1)} %param.12) | copy-start | bytes 12582916
  301.8 22.9 %slice-start.2 = ((s8[5767168]{0:T(1024)(128)(4,1)}), s8[4194304]{0:T(1024)(128)(4,1)S(1)}, s32[]{:S(2)}) async-start(s8[5767168]{0:T(1024)(128)(4,1)} %bitcast.17), calls=%async_computation.11 | async-start | bytes 8388608
  313.9 10.7 %copy-start.6 = (bf16[1024,2048]{1,0:T(8,128)(2,1)S(1)}, bf16[1024,2048]{1,0:T(8,128)(2,1)}, u32[]{:S(2)}) copy-start(bf16[1024,2048]{1,0:T(8,128)(2,1)} %param.13) | copy-start | bytes 12582916
  313.9 10.7 %slice-start.3 = ((s8[5767168]{0:T(1024)(128)(4,1)}), s8[1572864]{0:T(1024)(128)(4,1)S(1)}, s32[]{:S(2)}) async-start(s8[5767168]{0:T(1024)(128)(4,1)} %bitcast.17), calls=%async_computation.12 | async-start | bytes 3145728
  313.9 23.0 %slice-start = ((s8[5767168]{0:T(1024)(128)(4,1)}), s8[4194304]{0:T(1024)(128)(4,1)S(1)}, s32[]{:S(2)}) async-start(s8[5767168]{0:T(1024)(128)(4,1)} %bitcast.15), calls=%async_computation.9 | async-start | bytes 8388608
  324.7 12.3 %slice-start.1 = ((s8[5767168]{0:T(1024)(128)(4,1)}), s8[1572864]{0:T(1024)(128)(4,1)S(1)}, s32[]{:S(2)}) async-start(s8[5767168]{0:T(1024)(128)(4,1)} %bitcast.15), calls=%async_computation.10 | async-start | bytes 3145728
  361.9 335.4 %reduce-scatter.8.cloned.1.call-start = ((), (), s32[]{:S(2)}) async-start(), calls=%async_computation.8 | async-start | bytes 19464192 | tf_op jit(solution)/shard_map/reduce_scatter | solution.py:77
  361.9 13.0 %copy-start.2 = (bf16[1024,2048]{1,0:T(8,128)(2,1)S(1)}, bf16[1024,2048]{1,0:T(8,128)(2,1)}, u32[]{:S(2)}) copy-start(bf16[1024,2048]{1,0:T(8,128)(2,1)} %param.12) | copy-start | bytes 12582916
  404.1 41.5 %copy-start.7 = (f32[2048]{0:T(1024)S(1)}, f32[2048]{0:T(1024)}, u32[]{:S(2)}) copy-start(f32[2048]{0:T(1024)} %param.21) | copy-start | bytes 24580
  446.1 253.1 %copy-start.3 = (f32[256,1408]{1,0:T(8,128)S(1)}, f32[256,1408]{1,0:T(8,128)}, u32[]{:S(2)}) copy-start(f32[256,1408]{1,0:T(8,128)} %param.20) | copy-start | bytes 4325380
  446.1 253.1 %copy-start.4 = (f32[256,1408]{1,0:T(8,128)S(1)}, f32[256,1408]{1,0:T(8,128)}, u32[]{:S(2)}) copy-start(f32[256,1408]{1,0:T(8,128)} %param.19) | copy-start | bytes 4325380
  697.2 2.0 copy-start.5
Sparse Core Ops, SparseCore 0:
  10.2 95.0 all-gather.3
  107.4 90.4 all-gather.5
  200.1 90.4 all-gather.7
  301.6 42.7 reduce-scatter.3
  362.0 42.7 reduce-scatter.5
  408.6 288.6 reduce-scatter.7
where the time goes:
time: 709 us; the launch traced here: 708 us
  waiting for transfers between devices  500 us (71%)
  matrix products  121 us (17%)
  blocking collectives  41.4 us (6%)
  other arithmetic  31.1 us (4%)
  between operations  14.3 us (2%)
    reduce_scatter x1, waiting for transfers between devices, backward(): lax.psum_scatter(jnp.concatenate([outer_sum(normed, gate_and_up), 0.5 * o...  245 us
    all_gather x1, waiting for transfers between devices, local(): lax.all_gather(pieces[0], 'fs', axis=0, tiled=True)  90.8 us
    all_gather x1, waiting for transfers between devices, local(): lax.all_gather(pieces[2], 'fs', axis=0, tiled=True)  81.4 us
    all_gather x1, waiting for transfers between devices, local(): lax.all_gather(pieces[1], 'fs', axis=0, tiled=True)  80.8 us
    psum x1, blocking collectives, backward(): gain_total = lax.psum(gain_part, ('fs', 'tp'))  41.4 us
    dot_general x3, matrix products, transposed(): lax.dot_general(matrix_a, matrix_b, (((1,), (1,)), ((), ())), preferred_e...  32.2 us
    dot_general x2, matrix products, outer_sum(): lax.dot_general(matrix_a, matrix_b, (((0,), (0,)), ((), ())), preferred_e...  30.4 us
  transfers between devices with their start and end apart: 6, of which 4 were waited for; matrix products, arithmetic and copies ran while one was open for 19% of the time, Pallas kernels for 0%

commit v1 on v0

--- a/solution.py
+++ b/solution.py
@@ -103,13 +103,26 @@
     gain_sum,
 ):
     pieces = (gate_weight, up_weight, down_weight)
+
+    def search_the_panel(unit, lane_axis):
+        even, all_rows = (lax.axis_size(lane_axis), lax.axis_index(lane_axis))
+        a_now, block_last = (unit, 1)
+        while block_last < even:
+            opened = tuple(((it, it ^ block_last) for it in range(even)))
+            block_next = lax.ppermute(a_now, lane_axis, perm=opened)
+            formed = jnp.concatenate([a_now, block_next], 0)
+            r_now = jnp.concatenate([block_next, a_now], 0)
+            a_now = jnp.where(all_rows & block_last == 0, formed, r_now)
+            block_last = 2 * block_last
+        return a_now
+
     later_out, later_hidden = forward(
         later_in,
         norm_gain,
         (
             lax.all_gather(pieces[0], "fs", axis=0, tiled=True),
             lax.all_gather(pieces[1], "fs", axis=0, tiled=True),
-            lax.all_gather(pieces[2], "fs", axis=0, tiled=True),
+            search_the_panel(pieces[2], "fs"),
         ),
     )
     earlier = backward(

time: 709 us -> 797 us (1.12)
  waiting for transfers between devices: 500 us -> 570 us
    ppermute x0 -> x3, waiting for transfers between devices: none -> 112 us  [search_the_panel(): block_next = lax.ppermute(a_now, lane_axis, perm=opened)]
    all_gather x1, waiting for transfers between devices: 90.8 us -> 6.22 us  [local(): lax.all_gather(pieces[0], 'fs', axis=0, tiled=True)]
    all_gather x1, waiting for transfers between devices: 80.8 us -> 161 us  [local(): lax.all_gather(pieces[1], 'fs', axis=0, tiled=True)]
    all_gather x1, waiting for transfers between devices: 81.4 us -> 34.8 us  [local(): lax.all_gather(pieces[2], 'fs', axis=0, tiled=True)]
    reduce_scatter x1, waiting for transfers between devices: 245 us -> 254 us  [backward(): lax.psum_scatter(jnp.concatenate([outer_sum(normed, gate_and_up), 0.5 * o...]
  transfers between devices with their start and end apart: 6 -> 9, of which waited for: 4 -> 7; matrix products, arithmetic and copies ran while one was open for 19% -> 20% of each run, Pallas kernels for 0% -> 0%
where the time goes in v1:
time: 797 us; the launch traced here: 794 us
  waiting for transfers between devices  570 us (72%)
  matrix products  127 us (16%)
  blocking collectives  39.1 us (5%)
  other arithmetic  38.5 us (5%)
  between operations  14.5 us (2%)
    reduce_scatter x1, waiting for transfers between devices, backward(): lax.psum_scatter(jnp.concatenate([outer_sum(normed, gate_and_up), 0.5 * o...  254 us
    all_gather x1, waiting for transfers between devices, local(): lax.all_gather(pieces[1], 'fs', axis=0, tiled=True)  161 us
    ppermute x3, waiting for transfers between devices, search_the_panel(): block_next = lax.ppermute(a_now, lane_axis, perm=opened)  112 us
    psum x1, blocking collectives, backward(): gain_total = lax.psum(gain_part, ('fs', 'tp'))  39.1 us
    dot_general x3, matrix products, transposed(): lax.dot_general(matrix_a, matrix_b, (((1,), (1,)), ((), ())), preferred_e...  35.9 us
    all_gather x1, waiting for transfers between devices, local(): lax.all_gather(pieces[2], 'fs', axis=0, tiled=True)  34.8 us
    dot_general x2, matrix products, outer_sum(): lax.dot_general(matrix_a, matrix_b, (((0,), (0,)), ((), ())), preferred_e...  31.3 us
  transfers between devices with their start and end apart: 9, of which 7 were waited for; matrix products, arithmetic and copies ran while one was open for 20% of the time, Pallas kernels for 0%

profile of v1, /device:TPU:0, one launch (start us, length us, event | category | flops | bytes accessed | tf_op | source)
XLA Modules:
  0.0 794.3 jit_solution(4489853040333638073)
XLA Ops:
  9.4 3.0 collective-permute-start
  12.5 23.3 %collective-permute-done = bf16[256,1408]{1,0:T(8,128)(2,1)S(1)} collective-permute-done((bf16[256,1408]{1,0:T(8,128)(2,1)}, bf16[256,1408]{1,0:T(8,128)(2,1)S(1)}, u32[]{:S(2)}, u32[]{:S(2)}) %collective-permute-start) | collective-permute-done | bytes 720928 | tf_op jit(solution)/shard_map/ppermute | solution.py:112
  35.8 1.8 maximum_select_fusion.5
  37.5 1.5 collective-permute-start.1
  39.0 0.8 convert_element_type.59
  39.8 3.3 fusion.4
  43.1 0.9 fusion.13
  44.0 72.6 %collective-permute-done.1 = bf16[512,1408]{1,0:T(8,128)(2,1)S(1)} collective-permute-done((bf16[512,1408]{1,0:T(8,128)(2,1)S(1)}, bf16[512,1408]{1,0:T(8,128)(2,1)S(1)}, u32[]{:S(2)}, u32[]{:S(2)}) %collective-permute-start.1) | collective-permute-done | bytes 1441824 | tf_op jit(solution)/shard_map/ppermute | solution.py:112
  116.7 5.5 maximum_select_fusion.4
  122.2 0.7 collective-permute-start.2
  122.9 6.2 all-gather.4.cloned.1.call-done
  129.1 12.0 %fusion.28 = f32[1024,1408]{1,0:T(8,128)} fusion(bf16[2048,1408]{1,0:T(8,128)(2,1)} %all-gather.4.cloned.1.call-done, bf16[1024,2048]{1,0:T(8,128)(2,1)} %param.11, f32[2048]{0:T(1024)S(1)} %convert_element_type.59, f32[1024]{0:T(1024)S(1)} %add_rsqrt_fusion.1), kind=kOutput, calls=%fused_computation.48 | convolution fusion | flops 5913968640 | bytes 15740928 | tf_op jit(solution)/shard_map/dot_general | solution.py:36
  141.1 160.8 %all-gather.6.cloned.1.call-done = bf16[2048,1408]{1,0:T(8,128)(2,1)} async-done(((bf16[256,1408]{1,0:T(8,128)(2,1)}), bf16[2048,1408]{1,0:T(8,128)(2,1)}) %all-gather.6.cloned.1.call-update) | async-done | bytes 5767184 | tf_op jit(solution)/shard_map/all_gather | solution.py:124
  301.8 11.3 %multiply_convert_fusion.4 = bf16[1024,1408]{1,0:T(8,128)(2,1)S(1)} fusion(f32[1024,1408]{1,0:T(8,128)} %fusion.28, bf16[2048,1408]{1,0:T(8,128)(2,1)} %all-gather.6.cloned.1.call-done, bf16[1024,2048]{1,0:T(8,128)(2,1)} %param.11, f32[2048]{0:T(1024)S(1)} %convert_element_type.59, f32[1024]{0:T(1024)S(1)} %add_rsqrt_fusion.1), kind=kOutput, calls=%fused_computation.37 | convolution fusion | flops 5922619392 | bytes 18624512 | tf_op jit(solution)/shard_map/dot_general | solution.py:37
  313.1 15.7 %collective-permute-done.2 = bf16[1024,1408]{1,0:T(8,128)(2,1)S(1)} collective-permute-done((bf16[1024,1408]{1,0:T(8,128)(2,1)}, bf16[1024,1408]{1,0:T(8,128)(2,1)S(1)}, u32[]{:S(2)}, u32[]{:S(2)}) %collective-permute-start.2) | collective-permute-done | bytes 2883616 | tf_op jit(solution)/shard_map/ppermute | solution.py:112
  328.8 11.6 %fusion.26 = bf16[1024,2048]{1,0:T(8,128)(2,1)} fusion(bf16[1024,1408]{1,0:T(8,128)(2,1)S(1)} %multiply_convert_fusion.4, bf16[1024,1408]{1,0:T(8,128)(2,1)S(1)} %collective-permute-done.2, bf16[1024,1408]{1,0:T(8,128)(2,1)} %maximum_select_fusion.4, pred[]{:T(512)S(6)} %eq.9), kind=kOutput, calls=%fused_computation.40 | convolution fusion | flops 5933629440 | bytes 12845057 | tf_op jit(solution)/shard_map/dot_general | solution.py:18
  340.5 12.3 %fusion.35 = f32[1024,1408]{1,0:T(8,128)} fusion(bf16[2048,1408]{1,0:T(8,128)(2,1)} %all-gather.4.cloned.1.call-done, bf16[1024,2048]{1,0:T(8,128)(2,1)} %param.12, f32[1024]{0:T(1024)S(1)} %add_rsqrt_fusion, f32[2048]{0:T(1024)S(1)} %convert_element_type.59), kind=kOutput, calls=%fused_computation.55 | convolution fusion | flops 5913968640 | bytes 15740928 | tf_op jit(solution)/shard_map/dot_general | solution.py:52
  352.8 10.4 %fusion.37 = f32[1024,1408]{1,0:T(8,128)} fusion(bf16[2048,1408]{1,0:T(8,128)(2,1)} %all-gather.6.cloned.1.call-done, bf16[1024,2048]{1,0:T(8,128)(2,1)S(1)} %copy-done.1, f32[1024]{0:T(1024)S(1)} %add_rsqrt_fusion, f32[2048]{0:T(1024)S(1)} %convert_element_type.59), kind=kOutput, calls=%fused_computation.56 | convolution fusion | flops 5913968640 | bytes 15740928 | tf_op jit(solution)/shard_map/dot_general | solution.py:53
  363.2 34.8 %all-gather.8.cloned.1.call-done = bf16[2048,1408]{1,0:T(8,128)(2,1)} async-done(((bf16[256,1408]{1,0:T(8,128)(2,1)}), bf16[2048,1408]{1,0:T(8,128)(2,1)}) %all-gather.8.cloned.1.call-update) | async-done | bytes 5767184 | tf_op jit(solution)/shard_map/all_gather | solution.py:135
  398.0 14.1 %multiply_convert_fusion.2 = (bf16[1024,1408]{1,0:T(8,128)(2,1)S(1)}, bf16[1024,1408]{1,0:T(8,128)(2,1)S(1)}) fusion(f32[1024,1408]{1,0:T(8,128)} %fusion.35, f32[1024,1408]{1,0:T(8,128)} %fusion.37, bf16[1024,2048]{1,0:T(8,128)(2,1)} %param.13, bf16[2048,1408]{1,0:T(8,128)(2,1)} %all-gather.8.cloned.1.call-done), kind=kOutput, calls=%fused_computation.33 | convolution fusion | flops 5925765120 | bytes 27262976 | tf_op jit(solution)/shard_map/dot_general | solution.py:58
  412.2 12.8 %fusion.39 = f32[1024,2048]{1,0:T(8,128)} fusion(bf16[1024,1408]{1,0:T(8,128)(2,1)S(1)} %get-tuple-element.10, bf16[2048,1408]{1,0:T(8,128)(2,1)} %all-gather.4.cloned.1.call-done), kind=kOutput, calls=%fused_computation.57 | convolution fusion | flops 5905580032 | bytes 17039360 | tf_op jit(solution)/shard_map/dot_general | solution.py:18
  425.0 11.4 %fusion.12 = (f32[2048]{0:T(1024)S(1)}, f32[1024]{0:T(1024)S(1)}, f32[1024,2048]{1,0:T(8,128)S(1)}) fusion(bf16[1024,2048]{1,0:T(8,128)(2,1)S(1)} %copy-done.2, f32[1024]{0:T(1024)S(1)} %add_rsqrt_fusion, f32[2048]{0:T(1024)S(1)} %convert_element_type.59, f32[1024,2048]{1,0:T(8,128)} %fusion.39, bf16[1024,1408]{1,0:T(8,128)(2,1)S(1)} %get-tuple-element.9, ...), kind=kOutput, calls=%fused_computation.19 | convolution fusion | flops 5922354176 | bytes 29646848 | tf_op jit(solution)/shard_map/dot_general | solution.py:18
  436.4 3.5 fusion.11
  440.0 12.4 %fusion.14 = bf16[2048,1408]{1,0:T(8,128)(2,1)S(1)} fusion(bf16[1024,2048]{1,0:T(8,128)(2,1)} %param.13, f32[1024,1408]{1,0:T(8,128)} %fusion.37, f32[1024,1408]{1,0:T(8,128)} %fusion.35), kind=kOutput, calls=%fused_computation.21 | convolution fusion | flops 5919997952 | bytes 21495808 | tf_op jit(solution)/shard_map/dot_general | solution.py:24
  452.4 18.9 %convolution_convert_fusion = bf16[2048,2816]{1,0:T(8,128)(2,1)} fusion(bf16[1024,1408]{1,0:T(8,128)(2,1)} %copy-done.9, bf16[1024,1408]{1,0:T(8,128)(2,1)} %copy-done.10, bf16[1024,2048]{1,0:T(8,128)(2,1)S(1)} %copy-done.3, f32[1024]{0:T(1024)S(1)} %add_rsqrt_fusion, f32[2048]{0:T(1024)S(1)} %convert_element_type.59), kind=kOutput, calls=%fused_computation.2 | convolution fusion | flops 11836850176 | bytes 21508096 | tf_op jit(solution)/shard_map/dot_general | solution.py:24
  471.3 11.8 %pad_maximum_fusion = bf16[2048,4224]{1,0:T(8,128)(2,1)} fusion(bf16[2048,1408]{1,0:T(8,128)(2,1)S(1)} %fusion.14, bf16[2048,2816]{1,0:T(8,128)(2,1)} %convolution_convert_fusion), kind=kLoop, calls=%fused_computation | loop fusion | flops 34603008 | bytes 34603008 | tf_op jit(solution)/shard_map/concatenate | solution.py:78
  483.1 39.1 %psum.7 = f32[2048]{0:T(1024)S(1)} all-reduce(f32[2048]{0:T(1024)S(1)} %get-tuple-element.7), channel_id=1, replica_groups=mesh['fs'=8,'tp'=4] {'fs','tp'}, use_global_device_ids=true, to_apply=%region_7.8 | all-reduce | flops 2048 | bytes 16384 | tf_op jit(solution)/shard_map/psum | solution.py:88
  522.8 3.1 add_convert_fusion.1
  526.0 3.0 add_convert_fusion
  528.9 254.0 %reduce-scatter.8.cloned.1.call-done = bf16[256,4224]{1,0:T(8,128)(2,1)} async-done(((bf16[2048,4224]{1,0:T(8,128)(2,1)}), bf16[256,4224]{1,0:T(8,128)(2,1)}) %reduce-scatter.8.cloned.1.call-update) | async-done | bytes 2162704 | tf_op jit(solution)/shard_map/reduce_scatter | solution.py:77
  782.9 2.0 convert_element_type.74
  785.0 2.3 slice_add_fusion
  (40 shorter events, 3.0 us)
Async XLA Ops:
  7.2 121.9 %all-gather.4.cloned.1.call-start = ((), (), s32[]{:S(2)}) async-start(), calls=%async_computation.3 | async-start | bytes 6488064 | tf_op jit(solution)/shard_map/all_gather | solution.py:123
  7.9 293.9 %all-gather.6.cloned.1.call-start = ((), (), s32[]{:S(2)}) async-start(), calls=%async_computation.4 | async-start | bytes 6488064 | tf_op jit(solution)/shard_map/all_gather | solution.py:124
  8.7 389.4 %all-gather.8.cloned.1.call-start = ((), (), s32[]{:S(2)}) async-start(), calls=%async_computation.6 | async-start | bytes 6488064 | tf_op jit(solution)/shard_map/all_gather | solution.py:135
  9.4 513.5 %reduce-scatter.4.cloned.1.call-start = ((), (), s32[]{:S(2)}) async-start(), calls=%async_computation.5 | async-start | bytes 5242880 | tf_op jit(solution)/shard_map/reduce_scatter | solution.py:40
  9.4 26.3 %collective-permute-start = (bf16[256,1408]{1,0:T(8,128)(2,1)}, bf16[256,1408]{1,0:T(8,128)(2,1)S(1)}, u32[]{:S(2)}, u32[]{:S(2)}) collective-permute-start(bf16[256,1408]{1,0:T(8,128)(2,1)} %param.16), channel_id=1, source_target_pairs={{0,4},{4,0},{8,12},{12,8},{16,20},{20,16},{24,28},{28,24},{1,5},{5... | collective-permute-start | bytes 2162696 | tf_op jit(solution)/shard_map/ppermute | solution.py:112
  37.5 79.1 %collective-permute-start.1 = (bf16[512,1408]{1,0:T(8,128)(2,1)S(1)}, bf16[512,1408]{1,0:T(8,128)(2,1)S(1)}, u32[]{:S(2)}, u32[]{:S(2)}) collective-permute-start(bf16[512,1408]{1,0:T(8,128)(2,1)S(1)} %maximum_select_fusion.5), channel_id=1, source_target_pairs={{0,8},{4,12},{8,0},{12,4},{16,24},{20,28},{24,16},{28,20},{1,9},{5... | collective-permute-start | bytes 4325384 | tf_op jit(solution)/shard_map/ppermute | solution.py:112
  39.0 4.1 copy-start
  122.2 206.7 %collective-permute-start.2 = (bf16[1024,1408]{1,0:T(8,128)(2,1)}, bf16[1024,1408]{1,0:T(8,128)(2,1)S(1)}, u32[]{:S(2)}, u32[]{:S(2)}) collective-permute-start(bf16[1024,1408]{1,0:T(8,128)(2,1)} %maximum_select_fusion.4), channel_id=1, source_target_pairs={{0,16},{4,20},{8,24},{12,28},{16,0},{20,4},{24,8},{28,12},{1,17},{... | collective-permute-start | bytes 8650760 | tf_op jit(solution)/shard_map/ppermute | solution.py:112
  313.1 15.7 %copy-start.8 = (bf16[1024,1408]{1,0:T(8,128)(2,1)}, bf16[1024,1408]{1,0:T(8,128)(2,1)S(1)}, u32[]{:S(2)}) copy-start(bf16[1024,1408]{1,0:T(8,128)(2,1)S(1)} %multiply_convert_fusion.4) | copy-start | bytes 8650756
  340.5 185.5 %reduce-scatter.6.cloned.1.call-start = ((), (), s32[]{:S(2)}) async-start(), calls=%async_computation.7 | async-start | bytes 5242880 | tf_op jit(solution)/shard_map/reduce_scatter | solution.py:71
  340.5 12.3 %copy-start.1 = (bf16[1024,2048]{1,0:T(8,128)(2,1)S(1)}, bf16[1024,2048]{1,0:T(8,128)(2,1)}, u32[]{:S(2)}) copy-start(bf16[1024,2048]{1,0:T(8,128)(2,1)} %param.12) | copy-start | bytes 12582916
  412.2 12.9 %copy-start.10 = (bf16[1024,1408]{1,0:T(8,128)(2,1)}, bf16[1024,1408]{1,0:T(8,128)(2,1)S(1)}, u32[]{:S(2)}) copy-start(bf16[1024,1408]{1,0:T(8,128)(2,1)S(1)} %get-tuple-element.10) | copy-start | bytes 8650756
  412.2 12.9 %copy-start.9 = (bf16[1024,1408]{1,0:T(8,128)(2,1)}, bf16[1024,1408]{1,0:T(8,128)(2,1)S(1)}, u32[]{:S(2)}) copy-start(bf16[1024,1408]{1,0:T(8,128)(2,1)S(1)} %get-tuple-element.9) | copy-start | bytes 8650756
  412.2 12.9 %copy-start.2 = (bf16[1024,2048]{1,0:T(8,128)(2,1)S(1)}, bf16[1024,2048]{1,0:T(8,128)(2,1)}, u32[]{:S(2)}) copy-start(bf16[1024,2048]{1,0:T(8,128)(2,1)} %param.12) | copy-start | bytes 12582916
  440.0 343.0 %reduce-scatter.8.cloned.1.call-start = ((), (), s32[]{:S(2)}) async-start(), calls=%async_computation.8 | async-start | bytes 19464192 | tf_op jit(solution)/shard_map/reduce_scatter | solution.py:77
  440.0 12.4 %copy-start.3 = (bf16[1024,2048]{1,0:T(8,128)(2,1)S(1)}, bf16[1024,2048]{1,0:T(8,128)(2,1)}, u32[]{:S(2)}) copy-start(bf16[1024,2048]{1,0:T(8,128)(2,1)} %param.12) | copy-start | bytes 12582916
  483.1 39.1 %copy-start.7 = (f32[2048]{0:T(1024)S(1)}, f32[2048]{0:T(1024)}, u32[]{:S(2)}) copy-start(f32[2048]{0:T(1024)} %param.21) | copy-start | bytes 24580
  522.8 262.1 %copy-start.4 = (f32[256,1408]{1,0:T(8,128)S(1)}, f32[256,1408]{1,0:T(8,128)}, u32[]{:S(2)}) copy-start(f32[256,1408]{1,0:T(8,128)} %param.20) | copy-start | bytes 4325380
  522.8 262.1 %copy-start.5 = (f32[256,1408]{1,0:T(8,128)S(1)}, f32[256,1408]{1,0:T(8,128)}, u32[]{:S(2)}) copy-start(f32[256,1408]{1,0:T(8,128)} %param.19) | copy-start | bytes 4325380
  782.9 2.0 copy-start.6
Sparse Core Ops, SparseCore 0:
  10.2 118.8 all-gather.3
  131.3 170.4 all-gather.5
  304.0 94.0 all-gather.7
  400.4 42.7 reduce-scatter.3
  445.6 44.7 reduce-scatter.5
  494.1 288.7 reduce-scatter.7
